TPU v7x, 32 devices: a whole 2x2x4 slice. The times are simulated.
32 devices in a mesh: sp: 8 (over z, x), tp: 4 (over y, core).
Axes of the slice: x: 2, y: 2, z: 4, core: 2. Of those that a mesh axis runs over, the one named last changes fastest.
Arguments:
- tokens: bfloat16 [4, 8192, 2048], P(None, 'sp'), may hold values from -6 to 6
- norm_gain: bfloat16 [2048], replicated, may hold values from 0.099609375 to 1.8984375
- conv_value_weight: bfloat16 [2048, 1024], P('sp', 'tp'), may hold values from -0.125 to 0.125
- conv_gate_weight: bfloat16 [2048, 1024], P('sp', 'tp'), may hold values from -0.125 to 0.125
- query_weight: bfloat16 [2048, 1024], P('sp', 'tp'), may hold values from -40 to 40
- key_weight: bfloat16 [2048, 512], P('sp', 'tp'), may hold values from -1 to 1
- value_weight: bfloat16 [2048, 512], P('sp', 'tp'), may hold values from -0.125 to 0.125
- conv_taps: bfloat16 [31, 1024], P(None, 'tp'), may hold values from -1 to 1
- conv_gain: bfloat16 [1024], P('tp'), may hold values from 0.099609375 to 1.8984375
- sink_logit: float32 [16], P('tp'), may hold values from 1 to 6
- out_conv_weight: bfloat16 [1024, 2048], P('tp', 'sp'), may hold values from -0.125 to 0.125
- out_attn_weight: bfloat16 [1024, 2048], P('tp', 'sp'), may hold values from -0.125 to 0.125
Outputs:
- mixed: bfloat16 [4, 8192, 2048], P(None, ('sp', 'tp'))
- log_total: float32 [4, 16, 8192], P(None, 'tp', 'sp')
All inputs are finite; a program needn't handle non-finite values.
Results may differ from a plain program's by a relative error of at most 0.015.
Values may be sent and summed in bfloat16 or wider, within the bound.
A program may use at most 128 MiB of HBM per device.

v0:
```python
import functools
import math

import jax
import jax.numpy as jnp
from jax import lax
from jax.experimental import pallas as pl
from jax.experimental.pallas import tpu as pltpu
from jax.sharding import PartitionSpec as P

HEAD_DIM = 64
WINDOW = 128
LANES = 128
EPSILON = 1e-06
ROPE_BASE = 10000.0
MASK_VALUE = -1e30
F32 = jnp.float32
BF16 = jnp.bfloat16
VMEM_LIMIT = 60 * 1024 * 1024


def params(*semantics):
    return pltpu.CompilerParams(
        dimension_semantics=semantics, vmem_limit_bytes=VMEM_LIMIT
    )


def cost(flops, nbytes, trans=0):
    return pl.CostEstimate(flops=flops, bytes_accessed=nbytes, transcendentals=trans)


def ring_halo(value, width):
    size, length = lax.axis_size("sp"), value.shape[1]
    up = [(i, i + 1) for i in range(size - 1)]
    down = [(j, i) for i, j in up]
    before = lax.ppermute(value[:, length - width :], "sp", up)
    after = lax.ppermute(value[:, :width], "sp", down)
    return before, after


def gated_kernel(x_ref, w_ref, o_ref):
    ch = o_ref.shape[1]
    y = jnp.dot(x_ref[...], w_ref[...], preferred_element_type=F32)
    o_ref[...] = (y[:, :ch] * jax.nn.sigmoid(y[:, ch:])).astype(BF16)


def gated_proj(x, w):
    rows, width = x.shape
    ch = w.shape[1] // 2
    block = math.gcd(rows, 512)
    return pl.pallas_call(
        gated_kernel,
        grid=(rows // block,),
        in_specs=[
            pl.BlockSpec((block, width), lambda i: (i, 0)),
            pl.BlockSpec((width, 2 * ch), lambda i: (0, 0)),
        ],
        out_specs=pl.BlockSpec((block, ch), lambda i: (i, 0)),
        out_shape=jax.ShapeDtypeStruct((rows, ch), BF16),
        compiler_params=params("arbitrary"),
        cost_estimate=cost(4 * rows * width * ch, 2 * rows * width),
        name="gated_proj",
    )(x, w)


def qkv_kernel(qw, kw, x_ref, w_ref, cos_ref, sin_ref, q_ref, kv_ref):
    y = jnp.dot(x_ref[...], w_ref[...], preferred_element_type=F32)
    block = y.shape[0]
    cos, sin = cos_ref[...], sin_ref[...]
    lane = lax.broadcasted_iota(jnp.int32, (block, LANES), 1)
    low = lax.rem(lane, HEAD_DIM) < HEAD_DIM // 2
    for c in range(y.shape[1] // LANES):
        col = c * LANES
        part = y[:, col : col + LANES]
        if col < qw + kw:
            cs, sn = cos, sin
            if col + LANES > qw + kw:
                turned = lane + col < qw + kw
                cs, sn = jnp.where(turned, cs, 1.0), jnp.where(turned, sn, 0.0)
            half = HEAD_DIM // 2
            swap = jnp.where(
                low, pltpu.roll(part, LANES - half, 1), pltpu.roll(part, half, 1)
            )
            part = part * cs + swap * sn
        if col < qw:
            q_ref[:, col : col + LANES] = (part * HEAD_DIM ** (-0.5)).astype(BF16)
        else:
            kv_ref[:, col - qw : col - qw + LANES] = part.astype(BF16)


def qkv_proj(x, w, cos, sin, qw, kw):
    rows, width = x.shape
    tok = cos.shape[0]
    block = math.gcd(tok, 512)
    per_seq = tok // block
    return pl.pallas_call(
        functools.partial(qkv_kernel, qw, kw),
        grid=(rows // block,),
        in_specs=[
            pl.BlockSpec((block, width), lambda i: (i, 0)),
            pl.BlockSpec((width, w.shape[1]), lambda i: (0, 0)),
            pl.BlockSpec((block, LANES), lambda i: (i % per_seq, 0)),
            pl.BlockSpec((block, LANES), lambda i: (i % per_seq, 0)),
        ],
        out_specs=[
            pl.BlockSpec((block, qw), lambda i: (i, 0)),
            pl.BlockSpec((block, 2 * kw), lambda i: (i, 0)),
        ],
        out_shape=[
            jax.ShapeDtypeStruct((rows, qw), BF16),
            jax.ShapeDtypeStruct((rows, 2 * kw), BF16),
        ],
        compiler_params=params("arbitrary"),
        cost_estimate=cost(2 * rows * width * w.shape[1], 2 * rows * width),
        name="qkv_proj",
    )(x, w, cos, sin)


def conv_kernel(taps_n, halo, g_ref, b_ref, a_ref, t_ref, o_ref, xf):
    tok, ch = g_ref.shape[1], g_ref.shape[2]
    share = o_ref.shape[2]
    xf[0:halo] = b_ref[0].astype(F32)
    xf[halo : halo + tok] = g_ref[0].astype(F32)
    xf[halo + tok : halo + tok + halo] = a_ref[0].astype(F32)
    rows = math.gcd(share, 64)
    lead = halo - taps_n // 2

    def step(i, carry):
        base = pl.multiple_of(i * rows, rows)
        dest = base // share
        off = pl.multiple_of(lax.rem(base, share), rows)
        for lc in range(ch // LANES):
            ls = slice(lc * LANES, (lc + 1) * LANES)
            seg = xf[pl.ds(base, rows + 2 * halo), ls]
            total = None
            for r in range(8):
                part = None
                for a in range((2 * halo) // 8):
                    j = 8 * a + r - lead
                    if 0 <= j < taps_n:
                        need = rows + 8 if r else rows
                        piece = seg[8 * a : 8 * a + need] * t_ref[j : j + 1, ls]
                        part = piece if part is None else part + piece
                if part is None:
                    continue
                if r:
                    part = part[r : r + rows]
                total = part if total is None else total + part
            o_ref[dest, 0, pl.ds(off, rows), ls] = total.astype(BF16)
        return carry

    lax.fori_loop(0, tok // rows, step, 0)


def depthwise(gated, before, after, taps, tp):
    seqs, tok, ch = gated.shape
    halo = before.shape[1]
    share = tok // tp
    taps_n = taps.shape[0]
    return pl.pallas_call(
        functools.partial(conv_kernel, taps_n, halo),
        grid=(seqs,),
        in_specs=[
            pl.BlockSpec((1, tok, ch), lambda s: (s, 0, 0)),
            pl.BlockSpec((1, halo, ch), lambda s: (s, 0, 0)),
            pl.BlockSpec((1, halo, ch), lambda s: (s, 0, 0)),
            pl.BlockSpec((taps_n, ch), lambda s: (0, 0)),
        ],
        out_specs=pl.BlockSpec((tp, 1, share, ch), lambda s: (0, s, 0, 0)),
        out_shape=jax.ShapeDtypeStruct((tp, seqs, share, ch), BF16),
        scratch_shapes=[pltpu.VMEM((tok + 2 * halo, ch), F32)],
        compiler_params=params("arbitrary"),
        cost_estimate=cost(300 * seqs * tok * ch, 4 * seqs * tok * ch),
        name="depthwise",
    )(gated, before, after, taps)


def attn_kernel(
    group, sink_ref, q_ref, kv_ref, b_ref, a_ref, o_ref, l_ref, pad, kx, vt, bias
):
    tok, qw = q_ref.shape[1], q_ref.shape[2]
    kv2 = kv_ref.shape[2]
    kw = kv2 // 2
    share = o_ref.shape[2]
    heads = qw // HEAD_DIM
    rows = bias.shape[2]
    span = rows + 2 * WINDOW
    blocks = tok // rows
    length = tok + 2 * WINDOW

    @pl.when(pl.program_id(0) == 0)
    def _():
        offset = lax.axis_index("sp") * tok
        limit = tok * lax.axis_size("sp")
        key = lax.broadcasted_iota(jnp.int32, (span, rows), 0)
        rel = key - lax.broadcasted_iota(jnp.int32, (span, rows), 1)
        band = (rel >= 0) & (rel <= 2 * WINDOW)
        for b in range(blocks):
            pos = key + (offset + b * rows - WINDOW)
            ok = band & (pos >= 0) & (pos < limit)
            bias[b] = jnp.where(ok, 0.0, MASK_VALUE)

    pad[0:WINDOW] = b_ref[0]
    pad[WINDOW : WINDOW + tok] = kv_ref[0]
    pad[WINDOW + tok : length] = a_ref[0]
    lane = lax.broadcasted_iota(jnp.int32, (length, LANES), 1)
    for h in range(heads):
        at = (h * HEAD_DIM) % LANES
        src = (h // group) * HEAD_DIM
        chunk = src // LANES * LANES
        part = pad[:, chunk : chunk + LANES].astype(F32)
        shift = (at - src % LANES) % LANES
        if shift:
            part = pltpu.roll(part, shift, 1)
        keep = (lane >= at) & (lane < at + HEAD_DIM)
        kx[h] = jnp.where(keep, part, 0.0).astype(BF16)
    first = kw // LANES * LANES
    for c in range(first, kv2, LANES):
        vt[c - first : c - first + LANES] = (
            pad[:, c : c + LANES].astype(F32).T.astype(BF16)
        )

    for b in range(blocks):
        r0 = b * rows
        dest, off = r0 // share, r0 % share
        for pair in range(qw // LANES):
            q = q_ref[0, r0 : r0 + rows, pair * LANES : (pair + 1) * LANES]
            outs = []
            for h in range(pair * 2, pair * 2 + 2):
                sink = sink_ref[h]
                s = lax.dot_general(
                    kx[h, r0 : r0 + span],
                    q,
                    (((1,), (1,)), ((), ())),
                    preferred_element_type=F32,
                )
                s = s + bias[b]
                top = jnp.maximum(jnp.max(s, axis=0, keepdims=True), sink)
                e = jnp.exp(s - top)
                total = jnp.sum(e, axis=0, keepdims=True) + jnp.exp(sink - top)
                v0 = kw + (h // group) * HEAD_DIM - first
                o = jnp.dot(
                    vt[v0 : v0 + HEAD_DIM, r0 : r0 + span],
                    e.astype(BF16),
                    preferred_element_type=F32,
                )
                outs.append(o / total)
                l_ref[0, h : h + 1, r0 : r0 + rows] = top + jnp.log(total)
            both = jnp.concatenate(outs, axis=0).T
            o_ref[dest, 0, off : off + rows, pair * LANES : (pair + 1) * LANES] = (
                both.astype(BF16)
            )


def attention(q, kv, before, after, sink, tp):
    seqs, tok, qw = q.shape
    kv2 = kv.shape[2]
    kw = kv2 // 2
    heads = qw // HEAD_DIM
    group = heads // (kw // HEAD_DIM)
    share = tok // tp
    rows = math.gcd(share, 256)
    length = tok + 2 * WINDOW
    span = rows + 2 * WINDOW
    first = kw // LANES * LANES
    return pl.pallas_call(
        functools.partial(attn_kernel, group),
        grid=(seqs,),
        in_specs=[
            pl.BlockSpec(memory_space=pltpu.SMEM),
            pl.BlockSpec((1, tok, qw), lambda s: (s, 0, 0)),
            pl.BlockSpec((1, tok, kv2), lambda s: (s, 0, 0)),
            pl.BlockSpec((1, WINDOW, kv2), lambda s: (s, 0, 0)),
            pl.BlockSpec((1, WINDOW, kv2), lambda s: (s, 0, 0)),
        ],
        out_specs=[
            pl.BlockSpec((tp, 1, share, qw), lambda s: (0, s, 0, 0)),
            pl.BlockSpec((1, heads, tok), lambda s: (s, 0, 0)),
        ],
        out_shape=[
            jax.ShapeDtypeStruct((tp, seqs, share, qw), BF16),
            jax.ShapeDtypeStruct((seqs, heads, tok), F32),
        ],
        scratch_shapes=[
            pltpu.VMEM((length, kv2), BF16),
            pltpu.VMEM((heads, length, LANES), BF16),
            pltpu.VMEM((kv2 - first, length), BF16),
            pltpu.VMEM((tok // rows, span, rows), F32),
        ],
        compiler_params=params("arbitrary"),
        cost_estimate=cost(
            2000 * seqs * tok * qw, 8 * seqs * tok * qw, seqs * heads * tok * span
        ),
        name="attention",
    )(sink, q, kv, before, after)


def out_kernel(c_ref, a_ref, g_ref, w_ref, o_ref, x):
    tp, seqs, share, ch = c_ref.shape
    qw = a_ref.shape[3]
    step = ch + qw

    @pl.when(pl.program_id(0) == 0)
    def _():
        for s in range(seqs):
            parts = [c_ref[t, s].astype(F32) for t in range(tp)]
            mean = sum(p.sum(-1, keepdims=True) for p in parts) / (tp * ch)
            parts = [p - mean for p in parts]
            var = sum((p * p).sum(-1, keepdims=True) for p in parts) / (tp * ch)
            inv = lax.rsqrt(var + EPSILON)
            r = slice(s * share, (s + 1) * share)
            for t in range(tp):
                v = parts[t] * inv * g_ref[t].astype(F32)
                x[r, t * step : t * step + ch] = jax.nn.silu(v).astype(BF16)
                x[r, t * step + ch : (t + 1) * step] = a_ref[t, s]

    w = w_ref[0].reshape(tp * step, w_ref.shape[3])
    y = jnp.dot(x[...], w, preferred_element_type=F32).astype(BF16)
    o_ref[...] = y.reshape(o_ref.shape)


def out_proj(conv_tok, attn_tok, gain, weights):
    tp, seqs, share, ch = conv_tok.shape
    qw = attn_tok.shape[3]
    sp, _, depth, cols = weights.shape
    return pl.pallas_call(
        out_kernel,
        grid=(sp,),
        in_specs=[
            pl.BlockSpec((tp, seqs, share, ch), lambda j: (0, 0, 0, 0)),
            pl.BlockSpec((tp, seqs, share, qw), lambda j: (0, 0, 0, 0)),
            pl.BlockSpec((tp, 1, ch), lambda j: (0, 0, 0)),
            pl.BlockSpec((1, tp, depth, cols), lambda j: (j, 0, 0, 0)),
        ],
        out_specs=pl.BlockSpec((seqs, share, cols), lambda j: (0, 0, j)),
        out_shape=jax.ShapeDtypeStruct((seqs, share, sp * cols), BF16),
        scratch_shapes=[pltpu.VMEM((seqs * share, tp * depth), BF16)],
        compiler_params=params("arbitrary"),
        cost_estimate=cost(
            2 * seqs * share * tp * depth * sp * cols, 2 * sp * tp * depth * cols
        ),
        name="out_proj",
    )(conv_tok, attn_tok, gain, weights)


def on_device(
    tokens,
    norm_gain,
    conv_value_weight,
    conv_gate_weight,
    query_weight,
    key_weight,
    value_weight,
    conv_taps,
    conv_gain,
    sink_logit,
    out_conv_weight,
    out_attn_weight,
):
    seqs, tok, width = tokens.shape
    tp, sp = lax.axis_size("tp"), lax.axis_size("sp")
    ch = conv_value_weight.shape[1]
    qw, kw = query_weight.shape[1], key_weight.shape[1]

    conv_w = lax.all_gather(
        jnp.concatenate([conv_value_weight, conv_gate_weight], 1), "sp", axis=0, tiled=True
    )
    qkv_w = lax.all_gather(
        jnp.concatenate([query_weight, key_weight, value_weight], 1),
        "sp",
        axis=0,
        tiled=True,
    )
    out_w = lax.all_gather(
        jnp.concatenate([out_conv_weight, out_attn_weight], 0),
        ("sp", "tp"),
        axis=0,
        tiled=True,
    ).reshape(sp, tp, ch + qw, out_conv_weight.shape[1])
    gain = lax.all_gather(conv_gain.reshape(1, 1, ch), "tp", axis=0, tiled=True)

    floats = tokens.astype(F32)
    row_mean = floats.mean(-1, keepdims=True)
    centred = floats - row_mean
    variance = jnp.mean(centred * centred, -1, keepdims=True)
    normed = (centred * lax.rsqrt(variance + EPSILON) * norm_gain.astype(F32)).astype(BF16)
    normed = normed.reshape(seqs * tok, width)

    half = HEAD_DIM // 2
    lane = jnp.arange(LANES)
    inverse = ROPE_BASE ** (-(lane % half).astype(F32) / half)
    positions = (lax.axis_index("sp") * tok + jnp.arange(tok, dtype=jnp.int32)).astype(F32)
    angles = positions[:, None] * inverse[None, :]
    cos = jnp.cos(angles)
    sin = jnp.sin(angles) * jnp.where(lane % HEAD_DIM < half, -1.0, 1.0)[None, :]

    gated = gated_proj(normed, conv_w).reshape(seqs, tok, ch)
    halo = -(-(conv_taps.shape[0] // 2) // 16) * 16
    before, after = ring_halo(gated, halo)
    filtered = depthwise(gated, before, after, conv_taps.astype(F32), tp)
    conv_tok = lax.all_to_all(filtered, "tp", split_axis=0, concat_axis=0, tiled=True)

    q, kv = qkv_proj(normed, qkv_w, cos, sin, qw, kw)
    q, kv = q.reshape(seqs, tok, qw), kv.reshape(seqs, tok, 2 * kw)
    kv_before, kv_after = ring_halo(kv, WINDOW)
    attn_out, log_total = attention(q, kv, kv_before, kv_after, sink_logit, tp)
    attn_tok = lax.all_to_all(attn_out, "tp", split_axis=0, concat_axis=0, tiled=True)

    mixed = out_proj(conv_tok, attn_tok, gain, out_w)
    return (mixed, log_total)


def solution(mesh):
    placed = (
        P(None, "sp", None),
        P(),
        P("sp", "tp"),
        P("sp", "tp"),
        P("sp", "tp"),
        P("sp", "tp"),
        P("sp", "tp"),
        P(None, "tp"),
        P("tp"),
        P("tp"),
        P("tp", "sp"),
        P("tp", "sp"),
    )
    return jax.shard_map(
        on_device,
        mesh=mesh,
        in_specs=placed,
        out_specs=(P(None, ("sp", "tp"), None), P(None, "tp", "sp")),
        check_vma=False,
    )
```

profile of v0, /device:TPU:9, one launch (start us, length us, event | category | flops | bytes accessed | tf_op | source)
XLA Modules:
  0.0 233.6 jit_solution(6944158555578682484)
XLA Ops:
  7.2 0.0 all-gather.6.cloned.1.call-start
  7.2 1.7 pad_maximum_fusion
  8.9 0.0 all-gather.6.cloned.1.call-update
  8.9 0.0 all-gather.8.cloned.1.call-start
  9.0 1.7 pad_maximum_fusion.1
  10.7 0.0 all-gather.8.cloned.1.call-update
  10.7 0.0 all-gather.10.cloned.1.call-start
  10.8 1.7 pad_maximum_fusion.2
  12.4 0.0 all-gather.10.cloned.1.call-update
  12.5 0.7 convert_element_type.27
  13.2 0.0 copy-start
  13.2 7.2 %convert_reduce_fusion = f32[4,1024]{1,0:T(4,128)S(1)} fusion(bf16[4,1024,2048]{2,1,0:T(8,128)(2,1)} %param.12), kind=kLoop, calls=%fused_computation.1 | loop fusion | flops 16773120 | bytes 16793600 | tf_op jit(solution)/shard_map/reduce_sum | solution.py:383
  20.4 3.7 %copy-done = bf16[4,1024,2048]{2,1,0:T(8,128)(2,1)S(1)} copy-done((bf16[4,1024,2048]{2,1,0:T(8,128)(2,1)S(1)}, bf16[4,1024,2048]{2,1,0:T(8,128)(2,1)}, u32[]{:S(2)}) %copy-start) | copy-done | bytes 16777240
  24.1 5.5 %fusion.2 = f32[4,1024]{1,0:T(4,128)S(1)} fusion(bf16[4,1024,2048]{2,1,0:T(8,128)(2,1)S(1)} %copy-done, f32[4,1024]{1,0:T(4,128)S(1)} %broadcast_multiply_fusion), kind=kLoop, calls=%fused_computation.4 | loop fusion | flops 33550336 | bytes 16809984 | tf_op jit(solution)/shard_map/reduce_sum | solution.py:385
  29.6 8.8 %fusion.4 = bf16[4,1024,2048]{2,1,0:T(8,128)(2,1)} fusion(bf16[4,1024,2048]{2,1,0:T(8,128)(2,1)S(1)} %copy-done, f32[2048]{0:T(1024)S(1)} %convert_element_type.27, f32[4,1024]{1,0:T(4,128)S(1)} %add_rsqrt_fusion, f32[4,1024]{1,0:T(4,128)S(1)} %broadcast_multiply_fusion), kind=kLoop, calls=%fused_computation.6 | loop fusion | flops 41943040 | bytes 33595392 | tf_op jit(solution)/shard_map/convert_element_type | solution.py:386
  38.3 0.0 copy-start.4
  38.3 21.6 %all-gather.6.cloned.1.call-done.w_ref = bf16[2048,512]{1,0:T(8,128)(2,1)} async-done(((bf16[256,512]{1,0:T(8,128)(2,1)}), bf16[2048,512]{1,0:T(8,128)(2,1)}) %all-gather.6.cloned.1.call-update) | async-done | bytes 2097168 | tf_op jit(solution)/shard_map/all_gather | solution.py:365
  60.0 14.6 %gated_proj.1 = bf16[4096,256]{1,0:T(8,128)(2,1)} custom-call(bf16[4096,2048]{1,0:T(8,128)(2,1)} %bitcast.5, bf16[2048,512]{1,0:T(8,128)(2,1)} %all-gather.6.cloned.1.call-done.w_ref), custom_call_target="tpu_custom_call" | custom-call | flops 8589934592 | bytes 16777216 | tf_op jit(solution)/shard_map/gated_proj/pallas_call | solution.py:51
  74.6 0.8 fusion.11
  75.4 2.2 collective-permute-start
  77.6 3.9 %collective-permute-start.1 = (bf16[4,16,256]{2,1,0:T(8,128)(2,1)S(1)}, bf16[4,16,256]{2,1,0:T(8,128)(2,1)S(1)}, u32[]{:S(2)}, u32[]{:S(2)}) collective-permute-start(bf16[4,16,256]{2,1,0:T(8,128)(2,1)S(1)} %get-tuple-element.12), channel_id=1, source_target_pairs={{4,0},{8,4},{12,8},{16,12},{20,16},{24,20},{28,24},{5,1},{9,5},{13... | collective-permute-start | bytes 98312 | tf_op jit(solution)/shard_map/ppermute | solution.py:37
  81.6 0.0 copy-done.4
  81.6 0.6 convert_element_type.29.t_ref
  82.2 0.0 collective-permute-done.b_ref
  82.2 0.0 copy-start.2
  82.2 0.9 collective-permute-done.1.a_ref
  83.0 0.0 copy-done.2
  83.1 0.0 copy-start.3
  83.1 0.6 copy-done.3
  83.7 14.6 %depthwise.1 = bf16[4,4,256,256]{3,2,1,0:T(8,128)(2,1)} custom-call(bf16[4,1024,256]{2,1,0:T(8,128)(2,1)} %bitcast.8, bf16[4,16,256]{2,1,0:T(8,128)(2,1)} %copy-done.2, bf16[4,16,256]{2,1,0:T(8,128)(2,1)} %copy-done.3, f32[31,256]{1,0:T(8,128)} %convert_element_type.29.t_ref), custom_call_target="tpu_custom_call" | custom-call | flops 314572800 | bytes 4194304 | tf_op jit(solution)/shard_map/depthwise/pallas_call | solution.py:160
  98.3 6.0 %all-to-all-start = ((bf16[4,4,256,256]{3,2,1,0:T(8,128)(2,1)}), bf16[4,4,256,256]{3,2,1,0:T(8,128)(2,1)S(1)}, u32[]{:S(2)}, u32[]{:S(2)}) async-start(bf16[4,4,256,256]{3,2,1,0:T(8,128)(2,1)} %depthwise.1), calls=%async_computation | async-start | bytes 4194304 | tf_op jit(solution)/shard_map/all_to_all | solution.py:401
  104.3 3.1 %fusion.5 = (f32[1024,128]{1,0:T(8,128)}, f32[1024,128]{1,0:T(8,128)}) fusion(f32[128]{0:T(128)S(1)} %get-tuple-element.16, f32[128]{0:T(128)S(1)} %get-tuple-element.17, f32[1024]{0:T(1024)S(1)} %add_convert_fusion), kind=kLoop, calls=%fused_computation.9 | loop fusion | flops 262144 | bytes 1053696 | tf_op jit(solution)/shard_map/mul | solution.py:395
  107.4 2.6 %all-gather.8.cloned.1.call-done.w_ref = bf16[2048,512]{1,0:T(8,128)(2,1)} async-done(((bf16[256,512]{1,0:T(8,128)(2,1)}), bf16[2048,512]{1,0:T(8,128)(2,1)}) %all-gather.8.cloned.1.call-update) | async-done | bytes 2097168 | tf_op jit(solution)/shard_map/all_gather | solution.py:368
  110.0 17.1 %qkv_proj.1 = (bf16[4096,256]{1,0:T(8,128)(2,1)}, bf16[4096,256]{1,0:T(8,128)(2,1)}) custom-call(bf16[4096,2048]{1,0:T(8,128)(2,1)} %bitcast.6, bf16[2048,512]{1,0:T(8,128)(2,1)} %all-gather.8.cloned.1.call-done.w_ref, f32[1024,128]{1,0:T(8,128)} %get-tuple-element.15.cos_ref, f32[1024,128]{1,0:T(8,128)} %get-tuple-element.14.sin_ref), custom_call_target="tpu_custom_call" | custom-call | flops 8589934592 | bytes 16777216 | tf_op jit(solution)/shard_map/qkv_proj/pallas_call | solution.py:96
  127.1 0.0 copy-start.7
  127.1 1.1 fusion.10
  128.2 2.2 collective-permute-start.2
  130.4 4.0 %collective-permute-start.3 = (bf16[4,128,256]{2,1,0:T(8,128)(2,1)S(1)}, bf16[4,128,256]{2,1,0:T(8,128)(2,1)S(1)}, u32[]{:S(2)}, u32[]{:S(2)}) collective-permute-start(bf16[4,128,256]{2,1,0:T(8,128)(2,1)S(1)} %get-tuple-element.10), channel_id=1, source_target_pairs={{4,0},{8,4},{12,8},{16,12},{20,16},{24,20},{28,24},{5,1},{9,5},{13... | collective-permute-start | bytes 786440 | tf_op jit(solution)/shard_map/ppermute | solution.py:37
  134.4 4.2 %collective-permute-done.2.b_ref = bf16[4,128,256]{2,1,0:T(8,128)(2,1)S(1)} collective-permute-done((bf16[4,128,256]{2,1,0:T(8,128)(2,1)S(1)}, bf16[4,128,256]{2,1,0:T(8,128)(2,1)S(1)}, u32[]{:S(2)}, u32[]{:S(2)}) %collective-permute-start.2) | collective-permute-done | bytes 262176 | tf_op jit(solution)/shard_map/ppermute | solution.py:36
  138.5 0.0 copy-start.5
  138.5 9.5 %collective-permute-done.3.a_ref = bf16[4,128,256]{2,1,0:T(8,128)(2,1)S(1)} collective-permute-done((bf16[4,128,256]{2,1,0:T(8,128)(2,1)S(1)}, bf16[4,128,256]{2,1,0:T(8,128)(2,1)S(1)}, u32[]{:S(2)}, u32[]{:S(2)}) %collective-permute-start.3) | collective-permute-done | bytes 262176 | tf_op jit(solution)/shard_map/ppermute | solution.py:37
  148.1 0.0 copy-start.6
  148.1 0.0 copy-done.5
  148.1 0.7 copy-done.6
  148.8 29.8 %attention.1 = (bf16[4,4,256,256]{3,2,1,0:T(8,128)(2,1)}, f32[4,4,1024]{2,1,0:T(4,128)}) custom-call(f32[4]{0:T(128)} %sink_ref.1, bf16[4,1024,256]{2,1,0:T(8,128)(2,1)} %bitcast.12, bf16[4,1024,256]{2,1,0:T(8,128)(2,1)} %bitcast.10, bf16[4,128,256]{2,1,0:T(8,128)(2,1)} %copy-done.5, bf16[4,128,256]{2,1,0:T(8,128)(2,1)} %copy-done.6), custom_call_target="tpu_custom_call" | custom-call | flops 2097152000 | bytes 8388608 | tf_op jit(solution)/shard_map/attention/pallas_call | solution.py:266
  178.6 0.0 all-to-all-done.c_ref
  178.6 0.0 copy-start.1
  178.6 5.2 %all-to-all-start.1 = ((bf16[4,4,256,256]{3,2,1,0:T(8,128)(2,1)}), bf16[4,4,256,256]{3,2,1,0:T(8,128)(2,1)}, u32[]{:S(2)}, u32[]{:S(2)}) async-start(bf16[4,4,256,256]{3,2,1,0:T(8,128)(2,1)} %get-tuple-element.8), calls=%async_computation.1 | async-start | bytes 4194304 | tf_op jit(solution)/shard_map/all_to_all | solution.py:407
  183.8 0.0 copy-done.7
  183.8 26.8 %all-gather.1.g_ref = bf16[4,1,256]{2,1,0:T(2,128)(2,1)} all-gather(bf16[1,1,256]{2,1,0:T(2,128)(2,1)S(1)} %reshape.71), channel_id=2, replica_groups=mesh['sp'=8,'tp'=4] {'tp'}, dimensions={0}, use_global_device_ids=true | all-gather | bytes 2560 | tf_op jit(solution)/shard_map/all_gather | solution.py:380
  210.6 0.0 all-to-all-done.1.a_ref
  210.6 0.0 all-gather.10.cloned.1.call-done
  210.7 0.0 copy-done.1
  210.7 16.4 %out_proj.1 = bf16[4,256,2048]{2,1,0:T(8,128)(2,1)} custom-call(bf16[4,4,256,256]{3,2,1,0:T(8,128)(2,1)} %copy-done.1, bf16[4,4,256,256]{3,2,1,0:T(8,128)(2,1)} %all-to-all-done.1.a_ref, bf16[4,1,256]{2,1,0:T(2,128)(2,1)} %all-gather.1.g_ref, bf16[8,4,512,256]{3,2,1,0:T(8,128)(2,1)} %bitcast.11), custom_call_target="tpu_custom_call" | custom-call | flops 8589934592 | bytes 8388608 | tf_op jit(solution)/shard_map/out_proj/pallas_call | solution.py:326
  (5 shorter events, 0.0 us)
Async XLA Ops:
  7.2 52.8 %all-gather.6.cloned.1.call-start = ((), (), s32[]{:S(2)}) async-start(), calls=%async_computation.2 | async-start | bytes 2359296 | tf_op jit(solution)/shard_map/all_gather | solution.py:365
  8.9 101.0 %all-gather.8.cloned.1.call-start = ((), (), s32[]{:S(2)}) async-start(), calls=%async_computation.3 | async-start | bytes 2359296 | tf_op jit(solution)/shard_map/all_gather | solution.py:368
  10.7 199.9 %all-gather.10.cloned.1.call-start = ((), (), s32[]{:S(2)}) async-start(), calls=%async_computation.4 | async-start | bytes 8650752 | tf_op jit(solution)/shard_map/all_gather | solution.py:374
  13.2 10.9 %copy-start = (bf16[4,1024,2048]{2,1,0:T(8,128)(2,1)S(1)}, bf16[4,1024,2048]{2,1,0:T(8,128)(2,1)}, u32[]{:S(2)}) copy-start(bf16[4,1024,2048]{2,1,0:T(8,128)(2,1)} %param.12) | copy-start | bytes 50331652
  38.3 43.2 %copy-start.4 = (bf16[31,256]{1,0:T(8,128)(2,1)S(1)}, bf16[31,256]{1,0:T(8,128)(2,1)}, u32[]{:S(2)}) copy-start(bf16[31,256]{1,0:T(8,128)(2,1)} %param.19) | copy-start | bytes 47620
  75.4 6.8 %collective-permute-start = (bf16[4,16,256]{2,1,0:T(8,128)(2,1)S(1)}, bf16[4,16,256]{2,1,0:T(8,128)(2,1)S(1)}, u32[]{:S(2)}, u32[]{:S(2)}) collective-permute-start(bf16[4,16,256]{2,1,0:T(8,128)(2,1)S(1)} %get-tuple-element.13), channel_id=1, source_target_pairs={{0,4},{4,8},{8,12},{12,16},{16,20},{20,24},{24,28},{1,5},{5,9},{9,... | collective-permute-start | bytes 98312 | tf_op jit(solution)/shard_map/ppermute | solution.py:36
  77.6 5.4 %collective-permute-start.1 = (bf16[4,16,256]{2,1,0:T(8,128)(2,1)S(1)}, bf16[4,16,256]{2,1,0:T(8,128)(2,1)S(1)}, u32[]{:S(2)}, u32[]{:S(2)}) collective-permute-start(bf16[4,16,256]{2,1,0:T(8,128)(2,1)S(1)} %get-tuple-element.12), channel_id=1, source_target_pairs={{4,0},{8,4},{12,8},{16,12},{20,16},{24,20},{28,24},{5,1},{9,5},{13... | collective-permute-start | bytes 98312 | tf_op jit(solution)/shard_map/ppermute | solution.py:37
  82.2 0.9 copy-start.2
  83.1 0.6 copy-start.3
  98.3 80.3 %all-to-all-start = ((bf16[4,4,256,256]{3,2,1,0:T(8,128)(2,1)}), bf16[4,4,256,256]{3,2,1,0:T(8,128)(2,1)S(1)}, u32[]{:S(2)}, u32[]{:S(2)}) async-start(bf16[4,4,256,256]{3,2,1,0:T(8,128)(2,1)} %depthwise.1), calls=%async_computation | async-start | bytes 4194304 | tf_op jit(solution)/shard_map/all_to_all | solution.py:401
  127.1 56.7 %copy-start.7 = (bf16[256]{0:T(256)(128)(2,1)S(1)}, bf16[256]{0:T(256)(128)(2,1)}, u32[]{:S(2)}) copy-start(bf16[256]{0:T(256)(128)(2,1)} %param.20) | copy-start | bytes 1540
  128.2 10.4 %collective-permute-start.2 = (bf16[4,128,256]{2,1,0:T(8,128)(2,1)S(1)}, bf16[4,128,256]{2,1,0:T(8,128)(2,1)S(1)}, u32[]{:S(2)}, u32[]{:S(2)}) collective-permute-start(bf16[4,128,256]{2,1,0:T(8,128)(2,1)S(1)} %get-tuple-element.11), channel_id=1, source_target_pairs={{0,4},{4,8},{8,12},{12,16},{16,20},{20,24},{24,28},{1,5},{5,9},{9,... | collective-permute-start | bytes 786440 | tf_op jit(solution)/shard_map/ppermute | solution.py:36
  130.4 17.7 %collective-permute-start.3 = (bf16[4,128,256]{2,1,0:T(8,128)(2,1)S(1)}, bf16[4,128,256]{2,1,0:T(8,128)(2,1)S(1)}, u32[]{:S(2)}, u32[]{:S(2)}) collective-permute-start(bf16[4,128,256]{2,1,0:T(8,128)(2,1)S(1)} %get-tuple-element.10), channel_id=1, source_target_pairs={{4,0},{8,4},{12,8},{16,12},{20,16},{24,20},{28,24},{5,1},{9,5},{13... | collective-permute-start | bytes 786440 | tf_op jit(solution)/shard_map/ppermute | solution.py:37
  138.5 9.5 %copy-start.5 = (bf16[4,128,256]{2,1,0:T(8,128)(2,1)}, bf16[4,128,256]{2,1,0:T(8,128)(2,1)S(1)}, u32[]{:S(2)}) copy-start(bf16[4,128,256]{2,1,0:T(8,128)(2,1)S(1)} %collective-permute-done.2.b_ref) | copy-start | bytes 786436
  148.1 0.7 copy-start.6
  178.6 32.1 %copy-start.1 = (bf16[4,4,256,256]{3,2,1,0:T(8,128)(2,1)}, bf16[4,4,256,256]{3,2,1,0:T(8,128)(2,1)S(1)}, u32[]{:S(2)}) copy-start(bf16[4,4,256,256]{3,2,1,0:T(8,128)(2,1)S(1)} %all-to-all-done.c_ref) | copy-start | bytes 6291460
  178.6 32.0 %all-to-all-start.1 = ((bf16[4,4,256,256]{3,2,1,0:T(8,128)(2,1)}), bf16[4,4,256,256]{3,2,1,0:T(8,128)(2,1)}, u32[]{:S(2)}, u32[]{:S(2)}) async-start(bf16[4,4,256,256]{3,2,1,0:T(8,128)(2,1)} %get-tuple-element.8), calls=%async_computation.1 | async-start | bytes 4194304 | tf_op jit(solution)/shard_map/all_to_all | solution.py:407
Sparse Core Ops, SparseCore 0:
  10.7 49.2 all-gather.5
  62.1 47.8 all-gather.7
  112.8 80.7 all-gather.9
where the time goes:
time: 235 us; the launch traced here: 234 us
  Pallas kernels  92.5 us (39%)
  waiting for transfers between devices  38.8 us (17%)
  other arithmetic  30.9 us (13%)
  blocking collectives  26.8 us (11%)
  starting transfers between devices  23.7 us (10%)
  between operations  13.9 us (6%)
  local copies, waits for them, and re-layouts  6.93 us (3%)
    pallas_call x1, Pallas kernels, attention(): pl.pallas_call(functools.partial(attn_kernel, group), grid=(seqs,), in_sp...  29.8 us
    all_gather x1, blocking collectives, on_device(): gain = lax.all_gather(conv_gain.reshape(1, 1, ch), 'tp', axis=0, tiled=True)  26.8 us
    all_gather x1, waiting for transfers between devices, on_device(): lax.all_gather(jnp.concatenate([conv_value_weight, conv_gate_weight], 1),...  21.6 us
    pallas_call x1, Pallas kernels, qkv_proj(): pl.pallas_call(functools.partial(qkv_kernel, qw, kw), grid=(rows // block...  17.1 us
    pallas_call x1, Pallas kernels, out_proj(): pl.pallas_call(out_kernel, grid=(sp,), in_specs=[pl.BlockSpec((tp, seqs,...  16.4 us
    pallas_call x1, Pallas kernels, gated_proj(): pl.pallas_call(gated_kernel, grid=(rows // block,), in_specs=[pl.BlockSpe...  14.6 us
    pallas_call x1, Pallas kernels, depthwise(): pl.pallas_call(functools.partial(conv_kernel, taps_n, halo), grid=(seqs,)...  14.6 us
    ppermute x2, waiting for transfers between devices, ring_halo(): after = lax.ppermute(value[:, :width], 'sp', down)  10.4 us
  transfers between devices with their start and end apart: 9, of which 5 were waited for; matrix products, arithmetic and copies ran while one was open for 13% of the time, Pallas kernels for 33%

commit v1 on v0

--- a/solution.py
+++ b/solution.py
@@ -38,33 +38,12 @@
     return before, after
 
 
-def gated_kernel(x_ref, w_ref, o_ref):
-    ch = o_ref.shape[1]
-    y = jnp.dot(x_ref[...], w_ref[...], preferred_element_type=F32)
-    o_ref[...] = (y[:, :ch] * jax.nn.sigmoid(y[:, ch:])).astype(BF16)
-
-
-def gated_proj(x, w):
-    rows, width = x.shape
-    ch = w.shape[1] // 2
-    block = math.gcd(rows, 512)
-    return pl.pallas_call(
-        gated_kernel,
-        grid=(rows // block,),
-        in_specs=[
-            pl.BlockSpec((block, width), lambda i: (i, 0)),
-            pl.BlockSpec((width, 2 * ch), lambda i: (0, 0)),
-        ],
-        out_specs=pl.BlockSpec((block, ch), lambda i: (i, 0)),
-        out_shape=jax.ShapeDtypeStruct((rows, ch), BF16),
-        compiler_params=params("arbitrary"),
-        cost_estimate=cost(4 * rows * width * ch, 2 * rows * width),
-        name="gated_proj",
-    )(x, w)
-
-
-def qkv_kernel(qw, kw, x_ref, w_ref, cos_ref, sin_ref, q_ref, kv_ref):
-    y = jnp.dot(x_ref[...], w_ref[...], preferred_element_type=F32)
+def proj_kernel(qw, kw, x_ref, w_ref, cos_ref, sin_ref, g_ref, q_ref, kv_ref):
+    ch = g_ref.shape[1]
+    x = x_ref[...]
+    y = jnp.dot(x, w_ref[:, : 2 * ch], preferred_element_type=F32)
+    g_ref[...] = (y[:, :ch] * jax.nn.sigmoid(y[:, ch:])).astype(BF16)
+    y = jnp.dot(x, w_ref[:, 2 * ch :], preferred_element_type=F32)
     block = y.shape[0]
     cos, sin = cos_ref[...], sin_ref[...]
     lane = lax.broadcasted_iota(jnp.int32, (block, LANES), 1)
@@ -88,13 +67,13 @@
             kv_ref[:, col - qw : col - qw + LANES] = part.astype(BF16)
 
 
-def qkv_proj(x, w, cos, sin, qw, kw):
+def projections(x, w, cos, sin, ch, qw, kw):
     rows, width = x.shape
     tok = cos.shape[0]
     block = math.gcd(tok, 512)
     per_seq = tok // block
     return pl.pallas_call(
-        functools.partial(qkv_kernel, qw, kw),
+        functools.partial(proj_kernel, qw, kw),
         grid=(rows // block,),
         in_specs=[
             pl.BlockSpec((block, width), lambda i: (i, 0)),
@@ -103,16 +82,18 @@
             pl.BlockSpec((block, LANES), lambda i: (i % per_seq, 0)),
         ],
         out_specs=[
+            pl.BlockSpec((block, ch), lambda i: (i, 0)),
             pl.BlockSpec((block, qw), lambda i: (i, 0)),
             pl.BlockSpec((block, 2 * kw), lambda i: (i, 0)),
         ],
         out_shape=[
+            jax.ShapeDtypeStruct((rows, ch), BF16),
             jax.ShapeDtypeStruct((rows, qw), BF16),
             jax.ShapeDtypeStruct((rows, 2 * kw), BF16),
         ],
         compiler_params=params("arbitrary"),
         cost_estimate=cost(2 * rows * width * w.shape[1], 2 * rows * width),
-        name="qkv_proj",
+        name="projections",
     )(x, w, cos, sin)
 
 
@@ -252,8 +233,8 @@
             )
 
 
-def attention(q, kv, before, after, sink, tp):
-    seqs, tok, qw = q.shape
+def attention(q, kv, before, after, sink, tp, start, seqs):
+    _, tok, qw = q.shape
     kv2 = kv.shape[2]
     kw = kv2 // 2
     heads = qw // HEAD_DIM
@@ -268,10 +249,10 @@
         grid=(seqs,),
         in_specs=[
             pl.BlockSpec(memory_space=pltpu.SMEM),
-            pl.BlockSpec((1, tok, qw), lambda s: (s, 0, 0)),
-            pl.BlockSpec((1, tok, kv2), lambda s: (s, 0, 0)),
-            pl.BlockSpec((1, WINDOW, kv2), lambda s: (s, 0, 0)),
-            pl.BlockSpec((1, WINDOW, kv2), lambda s: (s, 0, 0)),
+            pl.BlockSpec((1, tok, qw), lambda s: (s + start, 0, 0)),
+            pl.BlockSpec((1, tok, kv2), lambda s: (s + start, 0, 0)),
+            pl.BlockSpec((1, WINDOW, kv2), lambda s: (s + start, 0, 0)),
+            pl.BlockSpec((1, WINDOW, kv2), lambda s: (s + start, 0, 0)),
         ],
         out_specs=[
             pl.BlockSpec((tp, 1, share, qw), lambda s: (0, s, 0, 0)),
@@ -295,9 +276,10 @@
     )(sink, q, kv, before, after)
 
 
-def out_kernel(c_ref, a_ref, g_ref, w_ref, o_ref, x):
+def out_kernel(c_ref, g_ref, w_ref, *rest):
+    *a_refs, o_ref, x = rest
     tp, seqs, share, ch = c_ref.shape
-    qw = a_ref.shape[3]
+    size, qw = a_refs[0].shape[1], a_refs[0].shape[3]
     step = ch + qw
 
     @pl.when(pl.program_id(0) == 0)
@@ -312,26 +294,26 @@
             for t in range(tp):
                 v = parts[t] * inv * g_ref[t].astype(F32)
                 x[r, t * step : t * step + ch] = jax.nn.silu(v).astype(BF16)
-                x[r, t * step + ch : (t + 1) * step] = a_ref[t, s]
+                x[r, t * step + ch : (t + 1) * step] = a_refs[s // size][t, s % size]
 
     w = w_ref[0].reshape(tp * step, w_ref.shape[3])
     y = jnp.dot(x[...], w, preferred_element_type=F32).astype(BF16)
     o_ref[...] = y.reshape(o_ref.shape)
 
 
-def out_proj(conv_tok, attn_tok, gain, weights):
+def out_proj(conv_tok, attn_parts, gain, weights):
     tp, seqs, share, ch = conv_tok.shape
-    qw = attn_tok.shape[3]
+    attn_shape = attn_parts[0].shape
     sp, _, depth, cols = weights.shape
     return pl.pallas_call(
         out_kernel,
         grid=(sp,),
         in_specs=[
             pl.BlockSpec((tp, seqs, share, ch), lambda j: (0, 0, 0, 0)),
-            pl.BlockSpec((tp, seqs, share, qw), lambda j: (0, 0, 0, 0)),
             pl.BlockSpec((tp, 1, ch), lambda j: (0, 0, 0)),
             pl.BlockSpec((1, tp, depth, cols), lambda j: (j, 0, 0, 0)),
-        ],
+        ]
+        + [pl.BlockSpec(attn_shape, lambda j: (0, 0, 0, 0))] * len(attn_parts),
         out_specs=pl.BlockSpec((seqs, share, cols), lambda j: (0, 0, j)),
         out_shape=jax.ShapeDtypeStruct((seqs, share, sp * cols), BF16),
         scratch_shapes=[pltpu.VMEM((seqs * share, tp * depth), BF16)],
@@ -340,7 +322,7 @@
             2 * seqs * share * tp * depth * sp * cols, 2 * sp * tp * depth * cols
         ),
         name="out_proj",
-    )(conv_tok, attn_tok, gain, weights)
+    )(conv_tok, gain, weights, *attn_parts)
 
 
 def on_device(
@@ -362,11 +344,10 @@
     ch = conv_value_weight.shape[1]
     qw, kw = query_weight.shape[1], key_weight.shape[1]
 
-    conv_w = lax.all_gather(
-        jnp.concatenate([conv_value_weight, conv_gate_weight], 1), "sp", axis=0, tiled=True
-    )
-    qkv_w = lax.all_gather(
-        jnp.concatenate([query_weight, key_weight, value_weight], 1),
+    in_w = lax.all_gather(
+        jnp.concatenate(
+            [conv_value_weight, conv_gate_weight, query_weight, key_weight, value_weight], 1
+        ),
         "sp",
         axis=0,
         tiled=True,
@@ -394,19 +375,29 @@
     cos = jnp.cos(angles)
     sin = jnp.sin(angles) * jnp.where(lane % HEAD_DIM < half, -1.0, 1.0)[None, :]
 
-    gated = gated_proj(normed, conv_w).reshape(seqs, tok, ch)
+    gated, q, kv = projections(normed, in_w, cos, sin, ch, qw, kw)
+    gated = gated.reshape(seqs, tok, ch)
+    q, kv = q.reshape(seqs, tok, qw), kv.reshape(seqs, tok, 2 * kw)
     halo = -(-(conv_taps.shape[0] // 2) // 16) * 16
     before, after = ring_halo(gated, halo)
+    kv_before, kv_after = ring_halo(kv, WINDOW)
     filtered = depthwise(gated, before, after, conv_taps.astype(F32), tp)
     conv_tok = lax.all_to_all(filtered, "tp", split_axis=0, concat_axis=0, tiled=True)
 
-    q, kv = qkv_proj(normed, qkv_w, cos, sin, qw, kw)
-    q, kv = q.reshape(seqs, tok, qw), kv.reshape(seqs, tok, 2 * kw)
-    kv_before, kv_after = ring_halo(kv, WINDOW)
-    attn_out, log_total = attention(q, kv, kv_before, kv_after, sink_logit, tp)
-    attn_tok = lax.all_to_all(attn_out, "tp", split_axis=0, concat_axis=0, tiled=True)
-
-    mixed = out_proj(conv_tok, attn_tok, gain, out_w)
+    attn_parts, totals = [], []
+    count = math.gcd(seqs, 2)
+    size = seqs // count
+    for part in range(count):
+        out, total = attention(
+            q, kv, kv_before, kv_after, sink_logit, tp, part * size, size
+        )
+        attn_parts.append(
+            lax.all_to_all(out, "tp", split_axis=0, concat_axis=0, tiled=True)
+        )
+        totals.append(total)
+    log_total = jnp.concatenate(totals, axis=0)
+
+    mixed = out_proj(conv_tok, attn_parts, gain, out_w)
     return (mixed, log_total)
 
 

time: 235 us -> 263 us (1.12)
  waiting for transfers between devices: 38.8 us -> 61.7 us
  local copies, waits for them, and re-layouts: 6.93 us -> 14.7 us
  Pallas kernels: 92.5 us -> 88.7 us
    all_gather x2 -> x1, waiting for transfers between devices: 24.2 us -> 41.1 us  [on_device(): lax.all_gather(jnp.concatenate([conv_value_weight, conv_gate_weight, quer...]
    unnamed x17 -> x29, local copies, waits for them, and re-layouts: 5.07 us -> 12 us
    pallas_call x2 -> x1, Pallas kernels: 31.7 us -> 25.6 us  [projections(): pl.pallas_call(functools.partial(proj_kernel, qw, kw), grid=(rows // bloc...]
    ppermute x2, waiting for transfers between devices: 4.16 us -> 9.36 us  [ring_halo(): before = lax.ppermute(value[:, length - width:], 'sp', up)]
    all_to_all x1 -> x2, starting transfers between devices: 5.19 us -> 8.33 us  [on_device(): lax.all_to_all(out, 'tp', split_axis=0, concat_axis=0, tiled=True)]
    pallas_call x1 -> x2, Pallas kernels: 29.8 us -> 32.2 us  [attention(): pl.pallas_call(functools.partial(attn_kernel, group), grid=(seqs,), in_sp...]
  transfers between devices with their start and end apart: 9 -> 9, of which waited for: 5 -> 5; matrix products, arithmetic and copies ran while one was open for 13% -> 12% of each run, Pallas kernels for 33% -> 28%
where the time goes in v1:
time: 263 us; the launch traced here: 260 us
  Pallas kernels  88.7 us (34%)
  waiting for transfers between devices  61.7 us (23%)
  other arithmetic  28.9 us (11%)
  blocking collectives  26.4 us (10%)
  starting transfers between devices  25.8 us (10%)
  local copies, waits for them, and re-layouts  14.7 us (6%)
  between operations  14.2 us (5%)
    all_gather x1, waiting for transfers between devices, on_device(): lax.all_gather(jnp.concatenate([conv_value_weight, conv_gate_weight, quer...  41.1 us
    pallas_call x2, Pallas kernels, attention(): pl.pallas_call(functools.partial(attn_kernel, group), grid=(seqs,), in_sp...  32.2 us
    all_gather x1, blocking collectives, on_device(): gain = lax.all_gather(conv_gain.reshape(1, 1, ch), 'tp', axis=0, tiled=True)  26.4 us
    pallas_call x1, Pallas kernels, projections(): pl.pallas_call(functools.partial(proj_kernel, qw, kw), grid=(rows // bloc...  25.6 us
    pallas_call x1, Pallas kernels, out_proj(): pl.pallas_call(out_kernel, grid=(sp,), in_specs=[pl.BlockSpec((tp, seqs,...  16.3 us
    pallas_call x1, Pallas kernels, depthwise(): pl.pallas_call(functools.partial(conv_kernel, taps_n, halo), grid=(seqs,)...  14.6 us
    unnamed x29, local copies, waits for them, and re-layouts  12 us
    ppermute x2, waiting for transfers between devices, ring_halo(): before = lax.ppermute(value[:, length - width:], 'sp', up)  9.36 us
  transfers between devices with their start and end apart: 9, of which 5 were waited for; matrix products, arithmetic and copies ran while one was open for 12% of the time, Pallas kernels for 28%

profile of v1, /device:TPU:9, one launch (start us, length us, event | category | flops | bytes accessed | tf_op | source)
XLA Modules:
  0.0 260.4 jit_solution(7274117186244667508)
XLA Ops:
  7.2 0.0 all-gather.5.cloned.1.call-start
  7.2 0.9 constant_dynamic-update-slice_fusion.4
  8.1 0.9 constant_dynamic-update-slice_fusion.3
  9.0 0.9 constant_dynamic-update-slice_fusion.2
  10.0 0.9 constant_dynamic-update-slice_fusion.1
  10.8 0.9 constant_dynamic-update-slice_fusion
  11.7 0.0 copy-start.4
  11.7 0.8 copy-done.4
  12.5 0.0 all-gather.5.cloned.1.call-update
  12.5 0.0 all-gather.7.cloned.1.call-start
  12.6 1.7 pad_maximum_fusion
  14.3 0.0 all-gather.7.cloned.1.call-update
  14.3 0.7 convert_element_type.27
  15.0 0.0 copy-start
  15.0 7.2 %convert_reduce_fusion = f32[4,1024]{1,0:T(4,128)S(1)} fusion(bf16[4,1024,2048]{2,1,0:T(8,128)(2,1)} %param.12), kind=kLoop, calls=%fused_computation.1 | loop fusion | flops 16773120 | bytes 16793600 | tf_op jit(solution)/shard_map/reduce_sum | solution.py:364
  22.2 4.0 %copy-done = bf16[4,1024,2048]{2,1,0:T(8,128)(2,1)S(1)} copy-done((bf16[4,1024,2048]{2,1,0:T(8,128)(2,1)S(1)}, bf16[4,1024,2048]{2,1,0:T(8,128)(2,1)}, u32[]{:S(2)}) %copy-start) | copy-done | bytes 16777240
  26.2 5.5 %fusion.2 = f32[4,1024]{1,0:T(4,128)S(1)} fusion(bf16[4,1024,2048]{2,1,0:T(8,128)(2,1)S(1)} %copy-done, f32[4,1024]{1,0:T(4,128)S(1)} %broadcast_multiply_fusion), kind=kLoop, calls=%fused_computation.4 | loop fusion | flops 33550336 | bytes 16809984 | tf_op jit(solution)/shard_map/reduce_sum | solution.py:366
  31.7 3.1 %fusion.5 = (f32[1024,128]{1,0:T(8,128)}, f32[1024,128]{1,0:T(8,128)}) fusion(f32[128]{0:T(128)S(1)} %get-tuple-element.22, f32[128]{0:T(128)S(1)} %get-tuple-element.23, f32[1024]{0:T(1024)S(1)} %add_convert_fusion), kind=kLoop, calls=%fused_computation.9 | loop fusion | flops 262144 | bytes 1053696 | tf_op jit(solution)/shard_map/mul | solution.py:376
  34.7 8.7 %fusion.4 = bf16[4,1024,2048]{2,1,0:T(8,128)(2,1)} fusion(bf16[4,1024,2048]{2,1,0:T(8,128)(2,1)S(1)} %copy-done, f32[2048]{0:T(1024)S(1)} %convert_element_type.27, f32[4,1024]{1,0:T(4,128)S(1)} %add_rsqrt_fusion, f32[4,1024]{1,0:T(4,128)S(1)} %broadcast_multiply_fusion), kind=kLoop, calls=%fused_computation.6 | loop fusion | flops 41943040 | bytes 33595392 | tf_op jit(solution)/shard_map/convert_element_type | solution.py:367
  43.5 41.1 %all-gather.5.cloned.1.call-done.w_ref = bf16[2048,1024]{1,0:T(8,128)(2,1)} async-done(((bf16[256,1024]{1,0:T(8,128)(2,1)}), bf16[2048,1024]{1,0:T(8,128)(2,1)}) %all-gather.5.cloned.1.call-update) | async-done | bytes 4194320 | tf_op jit(solution)/shard_map/all_gather | solution.py:347
  84.6 25.6 %projections.1 = (bf16[4096,256]{1,0:T(8,128)(2,1)}, bf16[4096,256]{1,0:T(8,128)(2,1)}, bf16[4096,256]{1,0:T(8,128)(2,1)}) custom-call(bf16[4096,2048]{1,0:T(8,128)(2,1)} %bitcast.5, bf16[2048,1024]{1,0:T(8,128)(2,1)} %all-gather.5.cloned.1.call-done.w_ref, f32[1024,128]{1,0:T(8,128)} %get-tuple-element.21.cos_ref, f32[1024,128]{1,0:T(8,128)} %get-tuple-element.20.sin_ref), custom_call_target="tpu_custom_call" | custom-call | flops 17179869184 | bytes 16777216 | tf_op jit(solution)/shard_map/projections/pallas_call | solution.py:75
  110.2 0.0 copy-start.8
  110.2 0.0 copy-start.11
  110.2 1.1 fusion.10
  111.3 2.2 collective-permute-start.2
  113.5 4.0 %collective-permute-start.3 = (bf16[4,128,256]{2,1,0:T(8,128)(2,1)S(1)}, bf16[4,128,256]{2,1,0:T(8,128)(2,1)S(1)}, u32[]{:S(2)}, u32[]{:S(2)}) collective-permute-start(bf16[4,128,256]{2,1,0:T(8,128)(2,1)S(1)} %get-tuple-element.16), channel_id=1, source_target_pairs={{4,0},{8,4},{12,8},{16,12},{20,16},{24,20},{28,24},{5,1},{9,5},{13... | collective-permute-start | bytes 786440 | tf_op jit(solution)/shard_map/ppermute | solution.py:37
  117.5 9.4 %collective-permute-done.2.b_ref = bf16[4,128,256]{2,1,0:T(8,128)(2,1)S(1)} collective-permute-done((bf16[4,128,256]{2,1,0:T(8,128)(2,1)S(1)}, bf16[4,128,256]{2,1,0:T(8,128)(2,1)S(1)}, u32[]{:S(2)}, u32[]{:S(2)}) %collective-permute-start.2) | collective-permute-done | bytes 262176 | tf_op jit(solution)/shard_map/ppermute | solution.py:36
  126.8 0.0 copy-start.9
  126.8 8.2 %collective-permute-done.3.a_ref = bf16[4,128,256]{2,1,0:T(8,128)(2,1)S(1)} collective-permute-done((bf16[4,128,256]{2,1,0:T(8,128)(2,1)S(1)}, bf16[4,128,256]{2,1,0:T(8,128)(2,1)S(1)}, u32[]{:S(2)}, u32[]{:S(2)}) %collective-permute-start.3) | collective-permute-done | bytes 262176 | tf_op jit(solution)/shard_map/ppermute | solution.py:37
  135.1 0.0 copy-start.10
  135.1 0.0 copy-done.9
  135.1 0.7 copy-done.10
  135.8 16.1 %attention.3 = (bf16[4,2,256,256]{3,2,1,0:T(8,128)(2,1)}, f32[2,4,1024]{2,1,0:T(4,128)}) custom-call(f32[4]{0:T(128)} %sink_ref.3, bf16[4,1024,256]{2,1,0:T(8,128)(2,1)} %bitcast.12, bf16[4,1024,256]{2,1,0:T(8,128)(2,1)} %bitcast.9, bf16[4,128,256]{2,1,0:T(8,128)(2,1)} %copy-done.9, bf16[4,128,256]{2,1,0:T(8,128)(2,1)} %copy-done.10), custom_call_target="tpu_custom_call" | custom-call | flops 1048576000 | bytes 4194304 | tf_op jit(solution)/shard_map/attention/pallas_call | solution.py:247
  151.9 0.0 copy-start.7
  151.9 4.4 %all-to-all-start.2 = ((bf16[4,2,256,256]{3,2,1,0:T(8,128)(2,1)}), bf16[4,2,256,256]{3,2,1,0:T(8,128)(2,1)S(1)}, u32[]{:S(2)}, u32[]{:S(2)}) async-start(bf16[4,2,256,256]{3,2,1,0:T(8,128)(2,1)} %get-tuple-element.13), calls=%async_computation.2 | async-start | bytes 2097152 | tf_op jit(solution)/shard_map/all_to_all | solution.py:395
  156.3 16.1 %attention.2 = (bf16[4,2,256,256]{3,2,1,0:T(8,128)(2,1)}, f32[2,4,1024]{2,1,0:T(4,128)}) custom-call(f32[4]{0:T(128)} %sink_ref.3, bf16[4,1024,256]{2,1,0:T(8,128)(2,1)} %bitcast.13, bf16[4,1024,256]{2,1,0:T(8,128)(2,1)} %bitcast.10, bf16[4,128,256]{2,1,0:T(8,128)(2,1)} %copy-done.9, bf16[4,128,256]{2,1,0:T(8,128)(2,1)} %copy-done.10), custom_call_target="tpu_custom_call" | custom-call | flops 1048576000 | bytes 4194304 | tf_op jit(solution)/shard_map/attention/pallas_call | solution.py:247
  172.4 2.0 all-to-all-done.2.rest_1_
  174.4 0.0 copy-start.2
  174.4 3.9 %all-to-all-start.1 = ((bf16[4,2,256,256]{3,2,1,0:T(8,128)(2,1)}), bf16[4,2,256,256]{3,2,1,0:T(8,128)(2,1)S(1)}, u32[]{:S(2)}, u32[]{:S(2)}) async-start(bf16[4,2,256,256]{3,2,1,0:T(8,128)(2,1)} %get-tuple-element.12), calls=%async_computation.1 | async-start | bytes 2097152 | tf_op jit(solution)/shard_map/all_to_all | solution.py:395
  178.4 0.8 fusion.11
  179.2 3.1 %collective-permute-start = (bf16[4,16,256]{2,1,0:T(8,128)(2,1)S(1)}, bf16[4,16,256]{2,1,0:T(8,128)(2,1)S(1)}, u32[]{:S(2)}, u32[]{:S(2)}) collective-permute-start(bf16[4,16,256]{2,1,0:T(8,128)(2,1)S(1)} %get-tuple-element.19), channel_id=1, source_target_pairs={{0,4},{4,8},{8,12},{12,16},{16,20},{20,24},{24,28},{1,5},{5,9},{9,... | collective-permute-start | bytes 98312 | tf_op jit(solution)/shard_map/ppermute | solution.py:36
  182.2 3.1 %collective-permute-start.1 = (bf16[4,16,256]{2,1,0:T(8,128)(2,1)S(1)}, bf16[4,16,256]{2,1,0:T(8,128)(2,1)S(1)}, u32[]{:S(2)}, u32[]{:S(2)}) collective-permute-start(bf16[4,16,256]{2,1,0:T(8,128)(2,1)S(1)} %get-tuple-element.18), channel_id=1, source_target_pairs={{4,0},{8,4},{12,8},{16,12},{20,16},{24,20},{28,24},{5,1},{9,5},{13... | collective-permute-start | bytes 98312 | tf_op jit(solution)/shard_map/ppermute | solution.py:37
  185.3 0.0 copy-done.8
  185.3 0.6 convert_element_type.31.t_ref
  186.0 0.0 collective-permute-done.b_ref
  186.0 0.0 copy-start.5
  186.0 0.9 collective-permute-done.1.a_ref
  186.9 0.0 copy-done.5
  186.9 0.0 copy-start.6
  186.9 0.6 copy-done.6
  187.5 14.6 %depthwise.1 = bf16[4,4,256,256]{3,2,1,0:T(8,128)(2,1)} custom-call(bf16[4,1024,256]{2,1,0:T(8,128)(2,1)} %bitcast.7, bf16[4,16,256]{2,1,0:T(8,128)(2,1)} %copy-done.5, bf16[4,16,256]{2,1,0:T(8,128)(2,1)} %copy-done.6, f32[31,256]{1,0:T(8,128)} %convert_element_type.31.t_ref), custom_call_target="tpu_custom_call" | custom-call | flops 314572800 | bytes 4194304 | tf_op jit(solution)/shard_map/depthwise/pallas_call | solution.py:141
  202.1 0.0 all-to-all-done.1.rest_0_
  202.1 0.0 copy-start.3
  202.1 1.0 copy-done.3
  203.1 5.0 %all-to-all-start = ((bf16[4,4,256,256]{3,2,1,0:T(8,128)(2,1)}), bf16[4,4,256,256]{3,2,1,0:T(8,128)(2,1)S(1)}, u32[]{:S(2)}, u32[]{:S(2)}) async-start(bf16[4,4,256,256]{3,2,1,0:T(8,128)(2,1)} %depthwise.1), calls=%async_computation | async-start | bytes 4194304 | tf_op jit(solution)/shard_map/all_to_all | solution.py:385
  208.1 0.0 copy-done.11
  208.1 26.4 %all-gather.1.g_ref = bf16[4,1,256]{2,1,0:T(2,128)(2,1)} all-gather(bf16[1,1,256]{2,1,0:T(2,128)(2,1)S(1)} %reshape.71), channel_id=2, replica_groups=mesh['sp'=8,'tp'=4] {'tp'}, dimensions={0}, use_global_device_ids=true | all-gather | bytes 2560 | tf_op jit(solution)/shard_map/all_gather | solution.py:361
  234.5 0.0 copy-done.7
  234.5 1.4 pad_maximum_fusion.1
  235.9 0.0 all-to-all-done.c_ref
  235.9 0.0 copy-start.1
  235.9 0.0 copy-done.2
  235.9 1.3 copy-done.1
  237.3 16.3 %out_proj.1 = bf16[4,256,2048]{2,1,0:T(8,128)(2,1)} custom-call(bf16[4,4,256,256]{3,2,1,0:T(8,128)(2,1)} %copy-done.1, bf16[4,1,256]{2,1,0:T(2,128)(2,1)} %all-gather.1.g_ref, bf16[8,4,512,256]{3,2,1,0:T(8,128)(2,1)} %bitcast.11, bf16[4,2,256,256]{3,2,1,0:T(8,128)(2,1)} %copy-done.3, bf16[4,2,256,256]{3,2,1,0:T(8,128)(2,1)} %copy-done.2), custom_call_target="tpu_custom_call" | custom-call | flops 8589934592 | bytes 8388608 | tf_op jit(solution)/shard_map/out_proj/pallas_call | solution.py:308
  (6 shorter events, 0.0 us)
Async XLA Ops:
  7.2 77.4 %all-gather.5.cloned.1.call-start = ((), (), s32[]{:S(2)}) async-start(), calls=%async_computation.3 | async-start | bytes 4718592 | tf_op jit(solution)/shard_map/all_gather | solution.py:347
  11.7 0.8 copy-start.4
  12.5 223.4 %all-gather.7.cloned.1.call-start = ((), (), s32[]{:S(2)}) async-start(), calls=%async_computation.4 | async-start | bytes 8650752 | tf_op jit(solution)/shard_map/all_gather | solution.py:355
  15.0 11.2 %copy-start = (bf16[4,1024,2048]{2,1,0:T(8,128)(2,1)S(1)}, bf16[4,1024,2048]{2,1,0:T(8,128)(2,1)}, u32[]{:S(2)}) copy-start(bf16[4,1024,2048]{2,1,0:T(8,128)(2,1)} %param.12) | copy-start | bytes 50331652
  110.2 75.2 %copy-start.8 = (bf16[31,256]{1,0:T(8,128)(2,1)S(1)}, bf16[31,256]{1,0:T(8,128)(2,1)}, u32[]{:S(2)}) copy-start(bf16[31,256]{1,0:T(8,128)(2,1)} %param.19) | copy-start | bytes 47620
  110.2 98.0 %copy-start.11 = (bf16[256]{0:T(256)(128)(2,1)S(1)}, bf16[256]{0:T(256)(128)(2,1)}, u32[]{:S(2)}) copy-start(bf16[256]{0:T(256)(128)(2,1)} %param.20) | copy-start | bytes 1540
  111.3 15.6 %collective-permute-start.2 = (bf16[4,128,256]{2,1,0:T(8,128)(2,1)S(1)}, bf16[4,128,256]{2,1,0:T(8,128)(2,1)S(1)}, u32[]{:S(2)}, u32[]{:S(2)}) collective-permute-start(bf16[4,128,256]{2,1,0:T(8,128)(2,1)S(1)} %get-tuple-element.17), channel_id=1, source_target_pairs={{0,4},{4,8},{8,12},{12,16},{16,20},{20,24},{24,28},{1,5},{5,9},{9,... | collective-permute-start | bytes 786440 | tf_op jit(solution)/shard_map/ppermute | solution.py:36
  113.5 21.6 %collective-permute-start.3 = (bf16[4,128,256]{2,1,0:T(8,128)(2,1)S(1)}, bf16[4,128,256]{2,1,0:T(8,128)(2,1)S(1)}, u32[]{:S(2)}, u32[]{:S(2)}) collective-permute-start(bf16[4,128,256]{2,1,0:T(8,128)(2,1)S(1)} %get-tuple-element.16), channel_id=1, source_target_pairs={{4,0},{8,4},{12,8},{16,12},{20,16},{24,20},{28,24},{5,1},{9,5},{13... | collective-permute-start | bytes 786440 | tf_op jit(solution)/shard_map/ppermute | solution.py:37
  126.8 8.2 %copy-start.9 = (bf16[4,128,256]{2,1,0:T(8,128)(2,1)}, bf16[4,128,256]{2,1,0:T(8,128)(2,1)S(1)}, u32[]{:S(2)}) copy-start(bf16[4,128,256]{2,1,0:T(8,128)(2,1)S(1)} %collective-permute-done.2.b_ref) | copy-start | bytes 786436
  135.1 0.7 copy-start.10
  151.9 82.6 %copy-start.7 = (f32[2,4,1024]{2,1,0:T(4,128)S(1)}, f32[2,4,1024]{2,1,0:T(4,128)}, u32[]{:S(2)}) copy-start(f32[2,4,1024]{2,1,0:T(4,128)} %get-tuple-element.15) | copy-start | bytes 98308
  151.9 22.5 %all-to-all-start.2 = ((bf16[4,2,256,256]{3,2,1,0:T(8,128)(2,1)}), bf16[4,2,256,256]{3,2,1,0:T(8,128)(2,1)S(1)}, u32[]{:S(2)}, u32[]{:S(2)}) async-start(bf16[4,2,256,256]{3,2,1,0:T(8,128)(2,1)} %get-tuple-element.13), calls=%async_computation.2 | async-start | bytes 2097152 | tf_op jit(solution)/shard_map/all_to_all | solution.py:395
  174.4 61.5 %copy-start.2 = (bf16[4,2,256,256]{3,2,1,0:T(8,128)(2,1)}, bf16[4,2,256,256]{3,2,1,0:T(8,128)(2,1)S(1)}, u32[]{:S(2)}) copy-start(bf16[4,2,256,256]{3,2,1,0:T(8,128)(2,1)S(1)} %all-to-all-done.2.rest_1_) | copy-start | bytes 3145732
  174.4 27.7 %all-to-all-start.1 = ((bf16[4,2,256,256]{3,2,1,0:T(8,128)(2,1)}), bf16[4,2,256,256]{3,2,1,0:T(8,128)(2,1)S(1)}, u32[]{:S(2)}, u32[]{:S(2)}) async-start(bf16[4,2,256,256]{3,2,1,0:T(8,128)(2,1)} %get-tuple-element.12), calls=%async_computation.1 | async-start | bytes 2097152 | tf_op jit(solution)/shard_map/all_to_all | solution.py:395
  179.2 6.8 %collective-permute-start = (bf16[4,16,256]{2,1,0:T(8,128)(2,1)S(1)}, bf16[4,16,256]{2,1,0:T(8,128)(2,1)S(1)}, u32[]{:S(2)}, u32[]{:S(2)}) collective-permute-start(bf16[4,16,256]{2,1,0:T(8,128)(2,1)S(1)} %get-tuple-element.19), channel_id=1, source_target_pairs={{0,4},{4,8},{8,12},{12,16},{16,20},{20,24},{24,28},{1,5},{5,9},{9,... | collective-permute-start | bytes 98312 | tf_op jit(solution)/shard_map/ppermute | solution.py:36
  182.2 4.7 %collective-permute-start.1 = (bf16[4,16,256]{2,1,0:T(8,128)(2,1)S(1)}, bf16[4,16,256]{2,1,0:T(8,128)(2,1)S(1)}, u32[]{:S(2)}, u32[]{:S(2)}) collective-permute-start(bf16[4,16,256]{2,1,0:T(8,128)(2,1)S(1)} %get-tuple-element.18), channel_id=1, source_target_pairs={{4,0},{8,4},{12,8},{16,12},{20,16},{24,20},{28,24},{5,1},{9,5},{13... | collective-permute-start | bytes 98312 | tf_op jit(solution)/shard_map/ppermute | solution.py:37
  186.0 0.9 copy-start.5
  186.9 0.6 copy-start.6
  202.1 1.0 copy-start.3
  203.1 32.8 %all-to-all-start = ((bf16[4,4,256,256]{3,2,1,0:T(8,128)(2,1)}), bf16[4,4,256,256]{3,2,1,0:T(8,128)(2,1)S(1)}, u32[]{:S(2)}, u32[]{:S(2)}) async-start(bf16[4,4,256,256]{3,2,1,0:T(8,128)(2,1)} %depthwise.1), calls=%async_computation | async-start | bytes 4194304 | tf_op jit(solution)/shard_map/all_to_all | solution.py:385
  235.9 1.3 copy-start.1
Sparse Core Ops, SparseCore 0:
  12.6 71.9 all-gather.4
  87.5 92.8 all-gather.6
